TPU v7x, 32 devices: a whole 2x2x4 slice. The times are simulated.
32 devices in a mesh: rep: 2 (over y), fs: 4 (over z), tp: 4 (over x, core).
Axes of the slice: x: 2, y: 2, z: 4, core: 2. Of those that a mesh axis runs over, the one named last changes fastest.
Arguments:
- tokens: bfloat16 [4096, 2048], P(('rep', 'fs')), may hold values from -6 to 6
- norm_gain: float32 [2048], replicated, may hold values from 0.1 to 1.9
- up_weight: bfloat16 [2048, 4096], P('fs', 'tp'), may hold values from -0.125 to 0.125
- down_weight: bfloat16 [4096, 2048], P('tp', 'fs'), may hold values from -0.09375 to 0.09375
Outputs:
- result: bfloat16 [4096, 2048], P(('rep', 'fs', 'tp'))
All inputs are finite; a program needn't handle non-finite values.
Results may differ from a plain program's by a relative error of at most 0.012.
Values may be sent and summed in bfloat16 or wider, within the bound.
A program may use at most 64 MiB of HBM per device.

v0:
```python
import functools

import jax
import jax.numpy as jnp
from jax import lax
from jax.experimental import pallas as pl
from jax.experimental.pallas import tpu as pltpu
from jax.sharding import PartitionSpec as P

EPS = 1e-06
UP_CHUNKS = 2
CHUNK_COLS = 128
LAG = 4


def shards(tokens, norm_gain, up_weight, down_weight):
    xf = tokens.astype(jnp.float32)
    scale = lax.rsqrt(jnp.mean(xf * xf, axis=-1, keepdims=True) + EPS)
    normed = (xf * scale * norm_gain).astype(jnp.bfloat16)
    rows = tokens.shape[0]
    halves = lax.axis_size("rep")
    share = up_weight.shape[0] // halves
    mine = lax.dynamic_slice_in_dim(up_weight, lax.axis_index("rep") * share, share, 0)
    arranged = normed.reshape(rows, -1, halves, share).transpose(0, 2, 1, 3).reshape(rows, -1)
    lifted = jnp.dot(
        arranged,
        lax.all_gather(mine, ("rep", "fs"), axis=0, tiled=True),
        preferred_element_type=jnp.float32,
    )
    width = down_weight.shape[1] // halves
    down_mine = lax.dynamic_slice_in_dim(down_weight, lax.axis_index("rep") * width, width, 1)
    collected = lax.all_gather(down_mine, ("rep", "fs"), axis=1, tiled=True)
    hidden_rows = collected.shape[0]
    down_block = (
        collected.reshape(hidden_rows, halves, -1, width)
        .transpose(0, 2, 1, 3)
        .reshape(hidden_rows, -1)
    )
    hidden = jnp.square(jnp.maximum(lifted, 0.0)).astype(jnp.bfloat16)
    own_rows = rows // lax.axis_size("tp")
    summed = lax.psum_scatter(
        jnp.dot(hidden, down_block, preferred_element_type=jnp.float32).astype(jnp.bfloat16),
        "tp",
        scatter_dimension=0,
        tiled=True,
    ).astype(jnp.float32)
    residual = lax.dynamic_slice_in_dim(xf, lax.axis_index("tp") * own_rows, own_rows, 0)
    return (residual + summed).astype(jnp.bfloat16)


def kernel(
    n, tok_hbm, gain_hbm, up_hbm, dn_hbm, out_hbm,
    gain_ref, tok, nrm, upw, dnw, hid, acc, keep, asend, arecv, bsend, brecv, outv,
    up_send, up_recv, dn_send, dn_recv, tok_send, tok_recv,
    a_send, a_recv, b_send, b_recv, local, out_sem,
):
    y, z, t = lax.axis_index("rep"), lax.axis_index("fs"), lax.axis_index("tp")
    x, core = t // 2, t % 2
    partner = x * 2 + (1 - core)
    rows = tok_hbm.shape[0]
    own_rows = rows // 4
    up_rows = up_hbm.shape[0]
    H = upw.shape[1]
    CW = dnw.shape[2]
    DC = dn_hbm.shape[1] // CW
    UC = UP_CHUNKS
    piece = up_rows // UC
    half = rows // 2
    total = n * DC

    def at(yy, zz, tt):
        return {"rep": yy, "fs": zz, "tp": tt}

    def remote(src, dst, send, recv, where):
        return pltpu.make_async_remote_copy(
            src_ref=src, dst_ref=dst, send_sem=send, recv_sem=recv,
            device_id=where, device_id_type=pl.DeviceIdType.MESH,
        )

    def beside(side):
        return at(y, z - 1 if side == 0 else z + 1, t)

    def up_slot(s, c):
        return upw.at[pl.ds(pl.multiple_of(s * up_rows + c * piece, piece), piece), :]

    def up_own(c):
        return up_hbm.at[pl.ds(c * piece, piece), pl.ds(pl.multiple_of(y * H, H), H)]

    def dn_own(c):
        return dn_hbm.at[pl.ds(pl.multiple_of(y * H, H), H), pl.ds(c * CW, CW)]

    def up_copy(side, s, c, src):
        return remote(src, up_slot(s, c), up_send.at[side, s * UC + c],
                      up_recv.at[s * UC + c], beside(side))

    def dn_copy(side, s, c, src):
        return remote(src, dnw.at[s * DC + c], dn_send.at[side, s * DC + c],
                      dn_recv.at[s * DC + c], beside(side))

    def dn_pair(side, s, c):
        two = dnw.at[pl.ds(s * DC + c, 2)]
        return remote(two, two, dn_send.at[side, s * DC + c], dn_recv.at[s * DC + c], beside(side))

    def outer(s):
        return (s == 0) | (s == n - 1)

    def send_own_dn(side):
        @pl.when(outer(z))
        def _():
            for c in range(DC):
                dn_copy(side, z, c, dnw.at[z * DC + c]).start()

        @pl.when(jnp.logical_not(outer(z)))
        def _():
            for c in range(0, DC, 2):
                dn_pair(side, z, c).start()

    def source(p):
        m = jnp.minimum(z, n - 1 - z)
        k = jnp.where(p <= 2 * m, (p + 1) // 2, p - m)
        sign = jnp.where(
            p <= 2 * m, jnp.where(p % 2 == 1, 1, -1), jnp.where(z < n - 1 - z, 1, -1)
        )
        return z + sign * k

    peers = [at(y, z, partner)]
    for j in (1, 2, 3):
        peers.append(at((y + j // 2) % 2, z, ((x + j % 2) % 2) * 2 + core))
    barrier = pltpu.get_barrier_semaphore()
    for peer in peers:
        pl.semaphore_signal(barrier, inc=1, device_id=peer, device_id_type=pl.DeviceIdType.MESH)
    has = (z > 0, z < n - 1)
    for side in (0, 1):
        @pl.when(has[side])
        def _():
            pl.semaphore_signal(
                barrier, inc=1, device_id=beside(side), device_id_type=pl.DeviceIdType.MESH
            )
    up_loads = [
        pltpu.make_async_copy(up_own(c), up_slot(z, c), local.at[c]) for c in range(UC)
    ]
    dn_loads = [
        pltpu.make_async_copy(dn_own(c), dnw.at[z * DC + c], local.at[UC + c]) for c in range(DC)
    ]
    tok_load = pltpu.make_async_copy(tok_hbm, tok.at[y], local.at[UC + DC])
    gain_load = pltpu.make_async_copy(gain_hbm, gain_ref, local.at[UC + DC + 1])
    for load in up_loads + dn_loads + [gain_load, tok_load]:
        load.start()

    greeted = 4 + jnp.where(has[0], 1, 0) + jnp.where(has[1], 1, 0)
    pl.semaphore_wait(barrier, greeted)

    for c in range(UC):
        up_loads[c].wait()
        for side in (0, 1):
            @pl.when(has[side])
            def _():
                up_copy(side, z, c, up_slot(z, c)).start()

    part = pl.ds(pl.multiple_of(core * half, half), half)
    across = remote(tok_hbm.at[part, :], tok.at[y, part, :], tok_send.at[0], tok_recv.at[0],
                    at(1 - y, z, t))
    across.start()
    for load in dn_loads:
        load.wait()

    @pl.when(z == 0)
    def _():
        send_own_dn(1)

    @pl.when(z == n - 1)
    def _():
        send_own_dn(0)

    gain_load.wait()
    gain = gain_ref[...]

    def normalise(yy):
        def tile(i, carry):
            xf = tok[yy, pl.ds(pl.multiple_of(i * own_rows, own_rows), own_rows), :].astype(jnp.float32)
            scale = lax.rsqrt(jnp.mean(xf * xf, axis=-1, keepdims=True) + EPS)
            to = (i % 2) * rows + (yy * 2 + i // 2) * own_rows
            nrm[pl.ds(pl.multiple_of(to, own_rows), own_rows), :] = (xf * scale * gain).astype(jnp.bfloat16)
            return carry
        lax.fori_loop(0, 4, tile, 0)

    tok_load.wait()
    normalise(y)

    for p in range(1, n):
        s = source(p)
        for c in range(UC):
            up_copy(0, s, c, up_slot(s, c)).wait_recv()
            for side in (0, 1):
                @pl.when(((s > z) if side == 0 else (s < z)) & has[side])
                def _():
                    up_copy(side, s, c, up_slot(s, c)).start()
        for side in (0, 1):
            @pl.when((s == (n - 1 if side == 0 else 0)) & has[side])
            def _():
                send_own_dn(side)

    theirs = pl.ds(pl.multiple_of((1 - core) * half, half), half)
    across.wait_recv()
    over = remote(tok.at[1 - y, part, :], tok.at[1 - y, part, :], tok_send.at[1], tok_recv.at[1],
                  at(y, z, partner))
    over.start()
    remote(tok.at[1 - y, theirs, :], tok.at[1 - y, theirs, :], tok_send.at[1], tok_recv.at[1],
           at(y, z, partner)).wait_recv()
    normalise(1 - y)

    def lift(i, carry):
        r = pl.ds(pl.multiple_of(i * half, half), half)
        lifted = jnp.dot(nrm[r, :], upw[...], preferred_element_type=jnp.float32)
        hid[r, :] = jnp.square(jnp.maximum(lifted, 0.0)).astype(jnp.bfloat16)
        return carry

    lax.fori_loop(0, 2 * rows // half, lift, 0)

    own_q = y * 2 + x

    def a_copy(i):
        return remote(asend.at[i], arecv.at[i], a_send.at[i], a_recv.at[i], at(y, z, partner))

    def b_copy(i, j):
        yy, xx = (y + j // 2) % 2, (x + j % 2) % 2
        return remote(bsend.at[i, yy * 2 + xx], brecv.at[i, j - 1], b_send.at[i, j - 1],
                      b_recv.at[i, j - 1], at(yy, z, xx * 2 + core))

    def out_copy(i):
        column = (source(i // DC) * DC + i % DC) * CW
        return pltpu.make_async_copy(
            outv.at[i], out_hbm.at[:, pl.ds(pl.multiple_of(column, CW), CW)], out_sem.at[i]
        )

    def finish(i):
        for j in (1, 2, 3):
            b_copy(i, j).wait_recv()
        column = (source(i // DC) * DC + i % DC) * CW
        res = tok[y, pl.ds(pl.multiple_of(t * own_rows, own_rows), own_rows),
                  pl.ds(pl.multiple_of(column, CW), CW)].astype(jnp.float32)
        res = res + keep[i]
        for j in range(3):
            res = res + brecv[i, j].astype(jnp.float32)
        outv[i] = res.astype(jnp.bfloat16)
        out_copy(i).start()

    def step(i, carry):
        p, c = i // DC, i % DC
        s = source(p)

        @pl.when((p > 0) & outer(s))
        def _():
            dn_copy(0, s, c, dnw.at[s * DC + c]).wait_recv()
            for side in (0, 1):
                @pl.when(((s > z) if side == 0 else (s < z)) & has[side])
                def _():
                    dn_copy(side, s, c, dnw.at[s * DC + c]).start()

        @pl.when((p > 0) & jnp.logical_not(outer(s)) & (c % 2 == 0))
        def _():
            dn_pair(0, s, c).wait_recv()
            for side in (0, 1):
                @pl.when(((s > z) if side == 0 else (s < z)) & has[side])
                def _():
                    dn_pair(side, s, c).start()

        block = dnw[s * DC + c]
        first = hid[pl.ds(pl.multiple_of((1 - core) * rows, rows), rows), :]
        asend[i] = jnp.dot(first, block, preferred_element_type=jnp.float32).astype(jnp.bfloat16)
        a_copy(i).start()
        second = hid[pl.ds(pl.multiple_of(core * rows, rows), rows), :]
        acc[i % 2] = jnp.dot(second, block, preferred_element_type=jnp.float32)

        @pl.when(i > 0)
        def _():
            join(i - 1)

        @pl.when(i >= LAG)
        def _():
            finish(i - LAG)
        return carry

    def join(i):
        a_copy(i).wait_recv()
        for q in range(4):
            r = pl.ds(q * own_rows, own_rows)
            bsend[i, q] = (acc[i % 2, r, :] + arecv[i, r, :].astype(jnp.float32)).astype(jnp.bfloat16)
        for j in (3, 2, 1):
            b_copy(i, j).start()
        r = pl.ds(pl.multiple_of(own_q * own_rows, own_rows), own_rows)
        keep[i] = acc[i % 2, r, :] + arecv[i, r, :].astype(jnp.float32)

    lax.fori_loop(0, total, step, 0)
    join(total - 1)
    for i in range(total - LAG, total - 1):
        finish(i)

    across.wait_send()
    over.wait_send()
    for side in (0, 1):
        for s in range(n):
            @pl.when(((z <= s) if side == 0 else (z >= s)) & has[side])
            def _():
                for c in range(UC):
                    up_copy(side, s, c, up_slot(s, c)).wait_send()
                if s in (0, n - 1):
                    for c in range(DC):
                        dn_copy(side, s, c, dnw.at[s * DC + c]).wait_send()
                else:
                    for c in range(0, DC, 2):
                        dn_pair(side, s, c).wait_send()

    def drain(i, carry):
        a_copy(i).wait_send()
        for j in (1, 2, 3):
            b_copy(i, j).wait_send()
        out_copy(i).wait()
        return carry

    lax.fori_loop(0, total - 1, drain, 0)
    finish(total - 1)
    drain(total - 1, 0)


def fused(n, tokens, norm_gain, up_weight, down_weight):
    rows, D = tokens.shape
    up_rows, block = up_weight.shape
    H = block // 2
    CW = CHUNK_COLS
    DC = down_weight.shape[1] // CW
    total = n * DC
    own_rows = rows // 4
    bf, f32 = jnp.bfloat16, jnp.float32
    dma = pltpu.SemaphoreType.DMA
    return pl.pallas_call(
        functools.partial(kernel, n),
        out_shape=jax.ShapeDtypeStruct((own_rows, D), bf),
        in_specs=[
            pl.BlockSpec(memory_space=pl.ANY),
            pl.BlockSpec(memory_space=pl.ANY),
            pl.BlockSpec(memory_space=pl.ANY),
            pl.BlockSpec(memory_space=pl.ANY),
        ],
        out_specs=pl.BlockSpec(memory_space=pl.ANY),
        scratch_shapes=[
            pltpu.VMEM((1, D), f32),
            pltpu.VMEM((2, rows, D), bf),
            pltpu.VMEM((2 * rows, D), bf),
            pltpu.VMEM((n * up_rows, H), bf),
            pltpu.VMEM((n * DC, H, CW), bf),
            pltpu.VMEM((2 * rows, H), bf),
            pltpu.VMEM((2, rows, CW), f32),
            pltpu.VMEM((total, own_rows, CW), f32),
            pltpu.VMEM((total, rows, CW), bf),
            pltpu.VMEM((total, rows, CW), bf),
            pltpu.VMEM((total, 4, own_rows, CW), bf),
            pltpu.VMEM((total, 3, own_rows, CW), bf),
            pltpu.VMEM((total, own_rows, CW), bf),
            dma((2, n * UP_CHUNKS)),
            dma((n * UP_CHUNKS,)),
            dma((2, n * DC)),
            dma((n * DC,)),
            dma((2,)),
            dma((2,)),
            dma((total,)),
            dma((total,)),
            dma((total, 3)),
            dma((total, 3)),
            dma((2 + UP_CHUNKS + DC,)),
            dma((total,)),
        ],
        compiler_params=pltpu.CompilerParams(
            collective_id=0, has_side_effects=True, vmem_limit_bytes=53 * 1024 * 1024
        ),
    )(tokens, norm_gain.reshape(1, D), up_weight, down_weight)


def fits(mesh, tokens, up_weight, down_weight):
    n = mesh.shape["fs"]
    rows = tokens.shape[0] // (mesh.shape["rep"] * n)
    columns = down_weight.shape[1] // n
    depth = up_weight.shape[0] // n
    hidden = up_weight.shape[1] // mesh.shape["tp"]
    return (
        mesh.shape["rep"] == 2
        and mesh.shape["tp"] == 4
        and n <= 8
        and columns % (2 * CHUNK_COLS) == 0
        and depth % (UP_CHUNKS * 16) == 0
        and hidden % 256 == 0
        and rows % 64 == 0
        and rows <= 512
        and hidden <= 1024
        and tokens.shape[1] <= 2048
    )


def solution(mesh):
    placed = (P(("rep", "fs"), None), P(), P("fs", "tp"), P("tp", "fs"))

    def layer(tokens, norm_gain, up_weight, down_weight):
        if fits(mesh, tokens, up_weight, down_weight):
            body = functools.partial(fused, mesh.shape["fs"])
        else:
            body = shards
        return jax.shard_map(
            body, mesh=mesh, in_specs=placed, out_specs=P(("rep", "fs", "tp"), None), check_vma=False
        )(tokens, norm_gain, up_weight, down_weight)

    return layer
```

profile of v0, /device:TPU:0, one launch (start us, length us, event | category | flops | bytes accessed | tf_op | source)
XLA Modules:
  0.0 82.6 jit_solution(11400334978404082824)
XLA Ops:
  0.0 0.0 copy-start
  0.0 0.7 copy-done
  0.7 81.1 %shard_map.46 = bf16[128,2048]{1,0:T(8,128)(2,1)S(1)} custom-call(bf16[512,2048]{1,0:T(8,128)(2,1)} %tok_hbm.1, f32[1,2048]{1,0:T(1,128)S(1)} %bitcast.1, bf16[512,1024]{1,0:T(8,128)(2,1)} %up_hbm.1, bf16[1024,512]{1,0:T(8,128)(2,1)} %dn_hbm.1), custom_call_target="tpu_custom_call" | custom-call | tf_op jit(solution)/shard_map/pallas_call | solution.py:336
  81.8 0.8 copy.6
Async XLA Ops:
  0.0 0.7 copy-start
where the time goes:
time: 82.8 us; the launch traced here: 82.6 us
  Pallas kernels  81.1 us (98%)
  local copies, waits for them, and re-layouts  1.49 us (2%)
    pallas_call x1, Pallas kernels, fused(): pl.pallas_call(functools.partial(kernel, n), out_shape=jax.ShapeDtypeStru...  81.1 us

commit v1 on v0

v1 whole, which is shorter than its diff:
```python
import functools

import jax
import jax.numpy as jnp
from jax import lax
from jax.experimental import pallas as pl
from jax.experimental.pallas import tpu as pltpu
from jax.sharding import PartitionSpec as P

EPS = 1e-06
UP_PIECES = 8
DN_CHUNKS = 2
DN_PIECES = 4
TOK_PIECES = 2
BESIDE = 2
LAG = 2


def shards(tokens, norm_gain, up_weight, down_weight):
    xf = tokens.astype(jnp.float32)
    scale = lax.rsqrt(jnp.mean(xf * xf, axis=-1, keepdims=True) + EPS)
    normed = (xf * scale * norm_gain).astype(jnp.bfloat16)
    rows = tokens.shape[0]
    halves = lax.axis_size("rep")
    share = up_weight.shape[0] // halves
    mine = lax.dynamic_slice_in_dim(up_weight, lax.axis_index("rep") * share, share, 0)
    arranged = normed.reshape(rows, -1, halves, share).transpose(0, 2, 1, 3).reshape(rows, -1)
    lifted = jnp.dot(
        arranged,
        lax.all_gather(mine, ("rep", "fs"), axis=0, tiled=True),
        preferred_element_type=jnp.float32,
    )
    width = down_weight.shape[1] // halves
    down_mine = lax.dynamic_slice_in_dim(down_weight, lax.axis_index("rep") * width, width, 1)
    collected = lax.all_gather(down_mine, ("rep", "fs"), axis=1, tiled=True)
    hidden_rows = collected.shape[0]
    down_block = (
        collected.reshape(hidden_rows, halves, -1, width)
        .transpose(0, 2, 1, 3)
        .reshape(hidden_rows, -1)
    )
    hidden = jnp.square(jnp.maximum(lifted, 0.0)).astype(jnp.bfloat16)
    own_rows = rows // lax.axis_size("tp")
    summed = lax.psum_scatter(
        jnp.dot(hidden, down_block, preferred_element_type=jnp.float32).astype(jnp.bfloat16),
        "tp",
        scatter_dimension=0,
        tiled=True,
    ).astype(jnp.float32)
    residual = lax.dynamic_slice_in_dim(xf, lax.axis_index("tp") * own_rows, own_rows, 0)
    return (residual + summed).astype(jnp.bfloat16)


def kernel(
    n, tok_hbm, gain_hbm, up_hbm, dn_hbm, out_hbm,
    gain_ref, tok, nrm, upw, dnw, lifted, hid, part, asend, arecv, bsend, brecv, keep, outv,
    up_send, up_recv, dn_send, dn_recv, t_send, t_recv,
    a_send, a_recv, b_send, b_recv, o_send, o_recv, local,
):
    y, z, t = lax.axis_index("rep"), lax.axis_index("fs"), lax.axis_index("tp")
    x, core = t // 2, t % 2
    rows = tok_hbm.shape[0]
    own_rows = rows // 4
    up_rows, H = up_hbm.shape
    CW = dnw.shape[2]
    UP, DC, DP, TP = UP_PIECES, DN_CHUNKS, DN_PIECES, TOK_PIECES
    UM, DM = UP // 2, DP // 2
    piece, depth, band = up_rows // UP, H // DP, own_rows // TP
    chunks = n * DC

    is_outer = (z == 0) | (z == n - 1)
    outer = jnp.where(z < n // 2, 0, n - 1)
    inner = jnp.where(z < n // 2, n // 2 - 1, n // 2)
    mate = n - 1 - z
    far = n - 1 - outer

    def at(yy, zz, tt):
        return {"rep": yy, "fs": zz, "tp": tt}

    PARTNER = at(y, z, x * 2 + (1 - core))
    ASIDE = at(y, z, (1 - x) * 2 + core)
    ACROSS = at(1 - y, z, t)
    MATE = at(y, mate, t)
    OUTER = at(y, outer, t)
    INNER = at(y, inner, t)

    def remote(src, dst, send, recv, where):
        return pltpu.make_async_remote_copy(
            src_ref=src, dst_ref=dst, send_sem=send, recv_sem=recv,
            device_id=where, device_id_type=pl.DeviceIdType.MESH,
        )

    def up_slot(s, p):
        return upw.at[pl.ds(pl.multiple_of(s * up_rows + p * piece, piece), piece), :]

    def up_own(p):
        return up_hbm.at[pl.ds(pl.multiple_of(p * piece, piece), piece), :]

    def dn_slot(s, j, k):
        return dnw.at[s * DC + j, pl.ds(pl.multiple_of(k * depth, depth), depth), :]

    def dn_own(j, k):
        return dn_hbm.at[pl.ds(pl.multiple_of(k * depth, depth), depth), pl.ds(j * CW, CW)]

    def up_copy(side, s, p, src, where):
        return remote(src, up_slot(s, p), up_send.at[side, s * UP + p], up_recv.at[s * UP + p], where)

    def dn_copy(side, s, j, k, src, where):
        q = (s * DC + j) * DP + k
        return remote(src, dn_slot(s, j, k), dn_send.at[side, q], dn_recv.at[q], where)

    def up_landed(s, p):
        up_copy(0, s, p, up_slot(s, p), MATE).wait_recv()

    def dn_landed(s, j, k):
        dn_copy(0, s, j, k, dn_slot(s, j, k), MATE).wait_recv()

    def tok_slot(q, b):
        return tok.at[1, pl.ds(pl.multiple_of(q * own_rows + b * band, band), band), :]

    def tok_copy(side, q, b, src, where):
        return remote(src, tok_slot(q, b), t_send.at[side, b], t_recv.at[side, b], where)

    def out_cols(s, j):
        return out_hbm.at[:, pl.ds(pl.multiple_of((s * DC + j) * CW, CW), CW)]

    barrier = pltpu.get_barrier_semaphore()

    def greet(peers):
        for peer in peers:
            pl.semaphore_signal(barrier, inc=1, device_id=peer, device_id_type=pl.DeviceIdType.MESH)

    mine_up, other_up = y * UM, (1 - y) * UM
    mine_dn, other_dn = y * DM, (1 - y) * DM

    @pl.when(is_outer)
    def _():
        greet([INNER])
        pl.semaphore_wait(barrier, 1)
        copies = []
        for p in range(UM):
            copies.append(up_copy(0, z, mine_up + p, up_own(mine_up + p), INNER))
        for b in range(TP):
            own = tok_hbm.at[pl.ds(pl.multiple_of(t * own_rows + b * band, band), band), :]
            copies.append(tok_copy(0, t, b, own, INNER))
        for p in range(UM - BESIDE):
            copies.append(up_copy(0, z, other_up + p, up_own(other_up + p), INNER))
        for first in (mine_dn, other_dn):
            for j in range(DC):
                for k in range(DM):
                    copies.append(dn_copy(0, z, j, first + k, dn_own(j, first + k), INNER))
        for copy in copies:
            copy.start()
        for copy in copies:
            copy.wait_send()
        for s in range(n):
            for j in range(DC):
                q = s * DC + j
                remote(outv.at[1, q], out_cols(s, j), o_send.at[q], o_recv.at[q], INNER).wait_recv()

    @pl.when(jnp.logical_not(is_outer))
    def _():
        greet([PARTNER, ASIDE, ACROSS, MATE, OUTER])
        tok_load = pltpu.make_async_copy(tok_hbm, tok.at[0], local.at[0])
        gain_load = pltpu.make_async_copy(gain_hbm, gain_ref, local.at[1])
        up_load = pltpu.make_async_copy(
            up_hbm, upw.at[pl.ds(pl.multiple_of(z * up_rows, up_rows), up_rows), :], local.at[2]
        )
        dn_loads = [
            pltpu.make_async_copy(dn_hbm.at[:, pl.ds(j * CW, CW)], dnw.at[z * DC + j], local.at[3 + j])
            for j in range(DC)
        ]
        for load in [gain_load, tok_load, up_load] + dn_loads:
            load.start()
        pl.semaphore_wait(barrier, 5)

        for p in range(UM):
            up_copy(0, z, mine_up + p, up_own(mine_up + p), MATE).start()

        gain_load.wait()
        gain = gain_ref[...]

        def normalise(src, q):
            xf = tok[src, pl.ds(pl.multiple_of(q * own_rows, own_rows), own_rows), :].astype(jnp.float32)
            scale = lax.rsqrt(jnp.mean(xf * xf, axis=-1, keepdims=True) + EPS)
            to = (q % 2 * 2 + q // 2) * own_rows
            nrm[src, pl.ds(pl.multiple_of(to, own_rows), own_rows), :] = (xf * scale * gain).astype(jnp.bfloat16)

        def lift(src, s, first=False, last=False):
            def half(i, carry):
                r = pl.ds(pl.multiple_of(i * (rows // 2), rows // 2), rows // 2)
                k = pl.ds(pl.multiple_of(s * up_rows, up_rows), up_rows)
                value = jnp.dot(nrm[src, r, k], upw[k, :], preferred_element_type=jnp.float32)
                if not first:
                    value = value + lifted[src, r, :]
                if last:
                    hid[src, i] = jnp.square(jnp.maximum(value, 0.0)).astype(jnp.bfloat16)
                else:
                    lifted[src, r, :] = value
                return carry
            lax.fori_loop(0, 2, half, 0)

        tok_load.wait()
        lax.fori_loop(0, 4, lambda q, carry: (normalise(0, q), carry)[1], 0)
        up_load.wait()

        def relay_near(p, carry):
            up_landed(outer, mine_up + p)
            up_copy(0, outer, mine_up + p, up_slot(outer, mine_up + p), MATE).start()

            @pl.when(p >= UM - BESIDE)
            def _():
                up_copy(1, outer, mine_up + p, up_slot(outer, mine_up + p), ACROSS).start()

            up_landed(mate, mine_up + p)
            up_copy(1, mate, mine_up + p, up_slot(mate, mine_up + p), ACROSS).start()
            return carry

        lax.fori_loop(0, 1, relay_near, 0)
        lift(0, z, first=True)
        lax.fori_loop(1, UM, relay_near, 0)
        for j in range(DC):
            dn_loads[j].wait()
            for k in range(DM):
                dn_copy(0, z, j, mine_dn + k, dn_own(j, mine_dn + k), MATE).start()

        def relay_far(p):
            up_landed(far, mine_up + p)
            up_copy(1, far, mine_up + p, up_slot(far, mine_up + p), ACROSS).start()

        beyond = (1 - x) * 2 + core
        for b in range(TP):
            for p in range(b * UM // TP, (b + 1) * UM // TP):
                relay_far(p)
            tok_copy(0, t, b, tok_slot(t, b), INNER).wait_recv()
            tok_copy(1, t, b, tok_slot(t, b), ASIDE).start()
            tok_copy(2, t, b, tok_slot(t, b), PARTNER).start()
        for p in range(UM):
            up_landed(mate, other_up + p)
        lift(0, mate)
        normalise(1, t)
        for b in range(TP):
            tok_copy(1, beyond, b, tok_slot(beyond, b), ASIDE).wait_recv()
            tok_copy(3, beyond, b, tok_slot(beyond, b), PARTNER).start()
        for b in range(TP):
            tok_copy(2, x * 2 + 1 - core, b, tok_slot(x * 2 + 1 - core, b), PARTNER).wait_recv()
        normalise(1, x * 2 + 1 - core)
        normalise(1, beyond)
        for b in range(TP):
            tok_copy(3, (1 - x) * 2 + 1 - core, b, tok_slot((1 - x) * 2 + 1 - core, b), PARTNER).wait_recv()
        normalise(1, (1 - x) * 2 + 1 - core)
        lift(1, z, first=True)
        lift(1, mate)
        for p in range(UM):
            up_landed(outer, other_up + p)
        lift(0, outer)

        def relay_dn(s, j, side, where):
            for k in range(DM):
                dn_landed(s, j, mine_dn + k)
                dn_copy(side, s, j, mine_dn + k, dn_slot(s, j, mine_dn + k), where).start()

        relay_dn(mate, 0, 1, ACROSS)
        lift(1, outer)
        for p in range(UM):
            up_landed(far, other_up + p)
        lift(0, far, last=True)
        lift(1, far, last=True)

        order = [(z, 0), (z, 1), (mate, 0), (mate, 1), (outer, 0), (far, 0), (outer, 1), (far, 1)]

        def a_copy(i):
            return remote(asend.at[i], arecv.at[i], a_send.at[i], a_recv.at[i], PARTNER)

        def b_copy(i):
            return remote(bsend.at[i], brecv.at[i], b_send.at[i], b_recv.at[i], ASIDE)

        def own_copy(i):
            s, j = order[i]
            return pltpu.make_async_copy(outv.at[0, s * DC + j], out_cols(s, j), local.at[3 + DC + i])

        def out_copy(i):
            s, j = order[i]
            q = s * DC + j
            return remote(outv.at[1, q], out_cols(s, j), o_send.at[q], o_recv.at[q], OUTER)

        def compute(i):
            s, j = order[i]
            block = dnw[s * DC + j]
            theirs = hid[:, 1 - core].reshape(rows, H)
            sent = jnp.dot(theirs, block, preferred_element_type=jnp.float32).astype(jnp.bfloat16)
            asend[i] = sent.reshape(2, 2, own_rows, CW)
            a_copy(i).start()
            ours = hid[:, core].reshape(rows, H)
            part[i % 2] = jnp.dot(ours, block, preferred_element_type=jnp.float32).reshape(2, 2, own_rows, CW)

        def join(i):
            a_copy(i).wait_recv()
            bsend[i] = (part[i % 2, :, 1 - x] + arecv[i, :, 1 - x].astype(jnp.float32)).astype(jnp.bfloat16)
            b_copy(i).start()
            keep[i] = part[i % 2, :, x] + arecv[i, :, x].astype(jnp.float32)

        def finish(i):
            s, j = order[i]
            q = s * DC + j
            b_copy(i).wait_recv()
            r = pl.ds(pl.multiple_of(t * own_rows, own_rows), own_rows)
            c = pl.ds(pl.multiple_of(q * CW, CW), CW)
            for src in (1, 0):
                res = tok[src, r, c].astype(jnp.float32) + keep[i, src] + brecv[i, src].astype(jnp.float32)
                outv[src, q] = res.astype(jnp.bfloat16)
                (own_copy if src == 0 else out_copy)(i).start()

        def arrive(s, j):
            for k in range(DM):
                dn_landed(s, j, other_dn + k)

        def own_arrive(s, j):
            for k in range(DM):
                dn_landed(s, j, mine_dn + k)

        before = {
            1: [lambda: relay_dn(mate, 1, 1, ACROSS), lambda: relay_dn(outer, 0, 0, MATE)],
            2: [lambda: arrive(mate, 0)],
            3: [lambda: relay_dn(outer, 1, 0, MATE), lambda: relay_dn(far, 0, 1, ACROSS), lambda: arrive(mate, 1)],
            4: [lambda: arrive(outer, 0)],
            5: [lambda: relay_dn(far, 1, 1, ACROSS), lambda: arrive(far, 0)],
            6: [lambda: arrive(outer, 1)],
            7: [lambda: arrive(far, 1)],
        }
        for i in range(chunks):
            for act in before.get(i, []):
                act()
            compute(i)
            if i > 0:
                join(i - 1)
            if i >= LAG:
                finish(i - LAG)
        join(chunks - 1)
        for i in range(chunks - LAG, chunks):
            finish(i)

        for p in range(UM):
            for side, s in ((0, z), (0, outer), (1, mate), (1, far)):
                up_copy(side, s, mine_up + p, up_slot(s, mine_up + p), MATE).wait_send()
            if p >= UM - BESIDE:
                up_copy(1, outer, mine_up + p, up_slot(outer, mine_up + p), MATE).wait_send()
        for b in range(TP):
            for side in (1, 2, 3):
                tok_copy(side, t, b, tok_slot(t, b), PARTNER).wait_send()
        for side, s in ((0, z), (0, outer), (1, mate), (1, far)):
            for j in range(DC):
                for k in range(DM):
                    dn_copy(side, s, j, mine_dn + k, dn_slot(s, j, mine_dn + k), MATE).wait_send()
        for i in range(chunks):
            a_copy(i).wait_send()
            b_copy(i).wait_send()
            own_copy(i).wait()
            out_copy(i).wait_send()


def fused(n, tokens, norm_gain, up_weight, down_weight):
    rows, D = tokens.shape
    up_rows, H = up_weight.shape
    CW = down_weight.shape[1] // DN_CHUNKS
    chunks = n * DN_CHUNKS
    own_rows = rows // 4
    bf, f32 = jnp.bfloat16, jnp.float32
    dma = pltpu.SemaphoreType.DMA
    return pl.pallas_call(
        functools.partial(kernel, n),
        out_shape=jax.ShapeDtypeStruct((own_rows, D), bf),
        in_specs=[pl.BlockSpec(memory_space=pl.ANY)] * 4,
        out_specs=pl.BlockSpec(memory_space=pl.ANY),
        scratch_shapes=[
            pltpu.VMEM((1, D), f32),
            pltpu.VMEM((2, rows, D), bf),
            pltpu.VMEM((2, rows, D), bf),
            pltpu.VMEM((n * up_rows, H), bf),
            pltpu.VMEM((chunks, H, CW), bf),
            pltpu.VMEM((2, rows, H), f32),
            pltpu.VMEM((2, 2, rows // 2, H), bf),
            pltpu.VMEM((2, 2, 2, own_rows, CW), f32),
            pltpu.VMEM((chunks, 2, 2, own_rows, CW), bf),
            pltpu.VMEM((chunks, 2, 2, own_rows, CW), bf),
            pltpu.VMEM((chunks, 2, own_rows, CW), bf),
            pltpu.VMEM((chunks, 2, own_rows, CW), bf),
            pltpu.VMEM((chunks, 2, own_rows, CW), f32),
            pltpu.VMEM((2, chunks, own_rows, CW), bf),
            dma((2, n * UP_PIECES)),
            dma((n * UP_PIECES,)),
            dma((2, chunks * DN_PIECES)),
            dma((chunks * DN_PIECES,)),
            dma((4, TOK_PIECES)),
            dma((4, TOK_PIECES)),
            dma((chunks,)),
            dma((chunks,)),
            dma((chunks,)),
            dma((chunks,)),
            dma((chunks,)),
            dma((chunks,)),
            dma((3 + DN_CHUNKS + chunks,)),
        ],
        compiler_params=pltpu.CompilerParams(
            collective_id=0, has_side_effects=True, vmem_limit_bytes=53 * 1024 * 1024
        ),
    )(tokens, norm_gain.reshape(1, D), up_weight, down_weight)


def fits(mesh, tokens, up_weight, down_weight):
    n = mesh.shape["fs"]
    rows = tokens.shape[0] // (mesh.shape["rep"] * n)
    columns = down_weight.shape[1] // n
    depth = up_weight.shape[0] // n
    hidden = up_weight.shape[1] // mesh.shape["tp"]
    return (
        mesh.shape["rep"] == 2
        and mesh.shape["tp"] == 4
        and n == 4
        and columns % (128 * DN_CHUNKS) == 0
        and depth % (UP_PIECES * 16) == 0
        and depth % 128 == 0
        and hidden % (16 * DN_PIECES) == 0
        and hidden % 128 == 0
        and rows % (4 * 16 * TOK_PIECES) == 0
        and rows <= 512
        and hidden <= 1024
        and tokens.shape[1] <= 2048
    )


def solution(mesh):
    placed = (P(("rep", "fs"), None), P(), P("fs", "tp"), P("tp", "fs"))

    def layer(tokens, norm_gain, up_weight, down_weight):
        if fits(mesh, tokens, up_weight, down_weight):
            body = functools.partial(fused, mesh.shape["fs"])
        else:
            body = shards
        return jax.shard_map(
            body, mesh=mesh, in_specs=placed, out_specs=P(("rep", "fs", "tp"), None), check_vma=False
        )(tokens, norm_gain, up_weight, down_weight)

    return layer
```

time: 82.8 us -> 82.8 us (level)
  no operation moved by 1% of the time
where the time goes in v1:
time: 82.8 us; the launch traced here: 82.6 us
  Pallas kernels  81.1 us (98%)
  local copies, waits for them, and re-layouts  1.49 us (2%)
    pallas_call x1, Pallas kernels, fused(): pl.pallas_call(functools.partial(kernel, n), out_shape=jax.ShapeDtypeStru...  81.1 us

profile of v1, /device:TPU:0, one launch (start us, length us, event | category | flops | bytes accessed | tf_op | source)
XLA Modules:
  0.0 82.6 jit_solution(18113171650745438805)
XLA Ops:
  0.0 0.0 copy-start
  0.0 0.7 copy-done
  0.7 81.1 %shard_map.46 = bf16[128,2048]{1,0:T(8,128)(2,1)S(1)} custom-call(bf16[512,2048]{1,0:T(8,128)(2,1)} %tok_hbm.1, f32[1,2048]{1,0:T(1,128)S(1)} %bitcast.1, bf16[512,1024]{1,0:T(8,128)(2,1)} %up_hbm.1, bf16[1024,512]{1,0:T(8,128)(2,1)} %dn_hbm.1), custom_call_target="tpu_custom_call" | custom-call | tf_op jit(solution)/shard_map/pallas_call | solution.py:370
  81.8 0.8 copy.6
Async XLA Ops:
  0.0 0.7 copy-start

commit v2 on v1

v2 whole, which is shorter than its diff:
```python
import functools

import jax
import jax.numpy as jnp
from jax import lax
from jax.experimental import pallas as pl
from jax.experimental.pallas import tpu as pltpu
from jax.sharding import PartitionSpec as P

EPS = 1e-06
UP_PIECES = 16
DN_CHUNKS = 2
DN_PIECES = 8
TOK_PIECES = 4
BESIDE = 4
VIA_MATE = 2
LAG = 4
ORDER = (
    ("inner", 0), ("inner", 1), ("mate", 0), ("mate", 1),
    ("outer", 0), ("far", 0), ("outer", 1), ("far", 1),
)
DIRECT = (1, 3, 5, 7)


def shards(tokens, norm_gain, up_weight, down_weight):
    xf = tokens.astype(jnp.float32)
    scale = lax.rsqrt(jnp.mean(xf * xf, axis=-1, keepdims=True) + EPS)
    normed = (xf * scale * norm_gain).astype(jnp.bfloat16)
    rows = tokens.shape[0]
    halves = lax.axis_size("rep")
    share = up_weight.shape[0] // halves
    mine = lax.dynamic_slice_in_dim(up_weight, lax.axis_index("rep") * share, share, 0)
    arranged = normed.reshape(rows, -1, halves, share).transpose(0, 2, 1, 3).reshape(rows, -1)
    lifted = jnp.dot(
        arranged,
        lax.all_gather(mine, ("rep", "fs"), axis=0, tiled=True),
        preferred_element_type=jnp.float32,
    )
    width = down_weight.shape[1] // halves
    down_mine = lax.dynamic_slice_in_dim(down_weight, lax.axis_index("rep") * width, width, 1)
    collected = lax.all_gather(down_mine, ("rep", "fs"), axis=1, tiled=True)
    hidden_rows = collected.shape[0]
    down_block = (
        collected.reshape(hidden_rows, halves, -1, width)
        .transpose(0, 2, 1, 3)
        .reshape(hidden_rows, -1)
    )
    hidden = jnp.square(jnp.maximum(lifted, 0.0)).astype(jnp.bfloat16)
    own_rows = rows // lax.axis_size("tp")
    summed = lax.psum_scatter(
        jnp.dot(hidden, down_block, preferred_element_type=jnp.float32).astype(jnp.bfloat16),
        "tp",
        scatter_dimension=0,
        tiled=True,
    ).astype(jnp.float32)
    residual = lax.dynamic_slice_in_dim(xf, lax.axis_index("tp") * own_rows, own_rows, 0)
    return (residual + summed).astype(jnp.bfloat16)


def kernel(
    n, tok_hbm, gain_hbm, up_hbm, dn_hbm, out_hbm,
    gain_ref, tok, nrm, upw, dnw, lifted, hid, part, asend, arecv, bsend, brecv, keep, outv, dsend, drecv,
    up_send, up_recv, dn_send, dn_recv, t_send, t_recv,
    a_send, a_recv, b_send, b_recv, o_send, o_recv, d_send, d_recv, own_sem, local,
):
    y, z, t = lax.axis_index("rep"), lax.axis_index("fs"), lax.axis_index("tp")
    x, core = t // 2, t % 2
    rows = tok_hbm.shape[0]
    own_rows = rows // 4
    up_rows, H = up_hbm.shape
    CW = dnw.shape[2]
    UP, DC, DP, TP = UP_PIECES, DN_CHUNKS, DN_PIECES, TOK_PIECES
    UM, DM = UP // 2, DP // 2
    piece, depth, band = up_rows // UP, H // DP, own_rows // TP
    chunks = n * DC

    is_outer = (z == 0) | (z == n - 1)
    outer = jnp.where(z < n // 2, 0, n - 1)
    inner = jnp.where(z < n // 2, n // 2 - 1, n // 2)
    mate = n - 1 - inner
    far = n - 1 - outer
    unit = {"inner": inner, "mate": mate, "outer": outer, "far": far}

    def at(yy, zz, tt):
        return {"rep": yy, "fs": zz, "tp": tt}

    PARTNER = at(y, z, x * 2 + (1 - core))
    ASIDE = at(y, z, (1 - x) * 2 + core)
    ACROSS = at(1 - y, z, t)
    MATE = at(y, mate, t)
    OUTER = at(y, outer, t)
    INNER = at(y, inner, t)

    def remote(src, dst, send, recv, where):
        return pltpu.make_async_remote_copy(
            src_ref=src, dst_ref=dst, send_sem=send, recv_sem=recv,
            device_id=where, device_id_type=pl.DeviceIdType.MESH,
        )

    def up_slot(s, p):
        return upw.at[pl.ds(pl.multiple_of(s * up_rows + p * piece, piece), piece), :]

    def up_own(p):
        return up_hbm.at[pl.ds(pl.multiple_of(p * piece, piece), piece), :]

    def dn_slot(s, j, k):
        return dnw.at[s * DC + j, pl.ds(pl.multiple_of(k * depth, depth), depth), :]

    def dn_own(j, k):
        return dn_hbm.at[pl.ds(pl.multiple_of(k * depth, depth), depth), pl.ds(j * CW, CW)]

    def up_copy(s, p, src, where, other=False):
        slot = up_slot(s, p + ((1 - y) if other else y) * UM)
        crossing = where is ACROSS or other
        recv = up_recv.at[n * UM + s] if crossing else up_recv.at[s * UM + p]
        return remote(slot if src is None else src, slot, up_send.at[0], recv, where)

    def dn_copy(s, j, k, src, where, other=False):
        slot = dn_slot(s, j, k + ((1 - y) if other else y) * DM)
        crossing = where is ACROSS or other
        recv = dn_recv.at[chunks * DM + s * DC + j] if crossing else dn_recv.at[(s * DC + j) * DM + k]
        return remote(slot if src is None else src, slot, dn_send.at[0], recv, where)

    def up_landed(s, p):
        up_copy(s, p, None, MATE).wait_recv()

    def up_others(s):
        half = up_rows // 2
        ref = upw.at[pl.ds(pl.multiple_of(s * up_rows + (1 - y) * half, half), half), :]
        remote(ref, ref, up_send.at[0], up_recv.at[n * UM + s], MATE).wait_recv()

    def dn_landed(s, j, k):
        dn_copy(s, j, k, None, MATE).wait_recv()

    def dn_others(s, j):
        half = H // 2
        ref = dnw.at[s * DC + j, pl.ds(pl.multiple_of((1 - y) * half, half), half), :]
        remote(ref, ref, dn_send.at[0], dn_recv.at[chunks * DM + s * DC + j], MATE).wait_recv()

    def tok_slot(q, b):
        return tok.at[1, pl.ds(pl.multiple_of(q * own_rows + b * band, band), band), :]

    def tok_copy(recv, q, b, src, where):
        return remote(src, tok_slot(q, b), t_send.at[0], t_recv.at[recv], where)

    def tok_all(recv, q):
        ref = tok.at[1, pl.ds(pl.multiple_of(q * own_rows, own_rows), own_rows), :]
        remote(ref, ref, t_send.at[0], t_recv.at[recv], MATE).wait_recv()

    def sent(ref, sem, where):
        remote(ref, ref, sem.at[0], sem.at[0], where).wait_send()

    def out_cols(q):
        return out_hbm.at[:, pl.ds(pl.multiple_of(q * CW, CW), CW)]

    def column(i):
        return unit[ORDER[i][0]] * DC + ORDER[i][1]

    def own_copy(i):
        q = column(i)
        return pltpu.make_async_copy(outv.at[0, q], out_cols(q), own_sem.at[0])

    def own_done(count):
        width = pl.ds(0, count * CW)
        pltpu.make_async_copy(tok.at[0, pl.ds(0, own_rows), width], out_hbm.at[:, width], own_sem.at[0]).wait()

    def out_copy(i):
        q = column(i)
        return remote(outv.at[1, q], out_cols(q), o_send.at[0], o_recv.at[i], OUTER)

    def d_copy(i, to, of):
        return remote(dsend.at[i, to], drecv.at[i, of], d_send.at[0], d_recv.at[i], at(y, outer, to * 2 + core))

    def d_landed(i):
        remote(dsend.at[i], drecv.at[i], d_send.at[0], d_recv.at[i], INNER).wait_recv()

    barrier = pltpu.get_barrier_semaphore()

    def greet(peers):
        for peer in peers:
            pl.semaphore_signal(barrier, inc=1, device_id=peer, device_id_type=pl.DeviceIdType.MESH)

    mine_up, other_up = y * UM, (1 - y) * UM
    mine_dn, other_dn = y * DM, (1 - y) * DM
    passed = len(DIRECT)
    own_block = pl.ds(pl.multiple_of(t * own_rows, own_rows), own_rows)

    def own_tokens(src, q):
        return tok[src, own_block, pl.ds(pl.multiple_of(q * CW, CW), CW)].astype(jnp.float32)

    @pl.when(is_outer)
    def _():
        greet([INNER, at(y, inner, (1 - x) * 2 + core)])
        load = pltpu.make_async_copy(tok_hbm.at[own_block, :], tok.at[0, own_block, :], local.at[0])
        load.start()
        up_load = pltpu.make_async_copy(
            up_hbm, upw.at[pl.ds(pl.multiple_of(z * up_rows, up_rows), up_rows), :], local.at[2]
        )
        up_load.start()
        pl.semaphore_wait(barrier, 2)
        up_load.wait()
        for p in range(UM):
            up_copy(z, p, None, INNER).start()
        for b in range(TP):
            own = tok_hbm.at[pl.ds(pl.multiple_of(t * own_rows + b * band, band), band), :]
            tok_copy(b, t, b, own, INNER).start()
        for p in range(UM - BESIDE):
            up_copy(z, p, None, INNER, True).start()
        for j in range(DC):
            for k in range(DM):
                dn_copy(z, j, k, dn_own(j, mine_dn + k), INNER).start()
        for j in range(DC):
            for k in range(DM):
                dn_copy(z, j, k, dn_own(j, other_dn + k), INNER, True).start()
        load.wait()
        for i in range(chunks):
            if i in DIRECT:
                d_landed(i)
                q = column(i)
                res = own_tokens(0, q) + drecv[i, 0].astype(jnp.float32) + drecv[i, 1].astype(jnp.float32)
                outv[0, q] = res.astype(jnp.bfloat16)
                own_copy(i).start()
            else:
                out_copy(i).wait_recv()
        sent(upw.at[pl.ds(0, (2 * UM - BESIDE) * piece), :], up_send, INNER)
        sent(dnw.at[pl.ds(0, DC)], dn_send, INNER)
        sent(tok.at[0, pl.ds(0, own_rows), :], t_send, INNER)
        own_done(passed)

    @pl.when(jnp.logical_not(is_outer))
    def _():
        greet([PARTNER, ASIDE, ACROSS, MATE, OUTER, at(y, outer, (1 - x) * 2 + core)])
        tok_load = pltpu.make_async_copy(tok_hbm, tok.at[0], local.at[0])
        gain_load = pltpu.make_async_copy(gain_hbm, gain_ref, local.at[1])
        up_load = pltpu.make_async_copy(
            up_hbm, upw.at[pl.ds(pl.multiple_of(z * up_rows, up_rows), up_rows), :], local.at[2]
        )
        dn_loads = [
            pltpu.make_async_copy(dn_hbm.at[:, pl.ds(j * CW, CW)], dnw.at[z * DC + j], local.at[3 + j])
            for j in range(DC)
        ]
        for load in [up_load, gain_load, tok_load] + dn_loads:
            load.start()
        pl.semaphore_wait(barrier, 6)

        up_load.wait()
        for p in range(UM):
            up_copy(z, p, None, MATE).start()

        gain_load.wait()
        gain = gain_ref[...]

        def normalise(src, q):
            xf = tok[src, pl.ds(pl.multiple_of(q * own_rows, own_rows), own_rows), :].astype(jnp.float32)
            scale = lax.rsqrt(jnp.mean(xf * xf, axis=-1, keepdims=True) + EPS)
            to = (q % 2 * 2 + q // 2) * own_rows
            nrm[src, pl.ds(pl.multiple_of(to, own_rows), own_rows), :] = (xf * scale * gain).astype(jnp.bfloat16)

        def lift(src, start, size, first=False, last=False):
            k = pl.ds(pl.multiple_of(start, size), size)
            value = jnp.dot(nrm[src, :, k], upw[k, :], preferred_element_type=jnp.float32)
            if not first:
                value = value + lifted[src]
            if last:
                hid[src] = jnp.square(jnp.maximum(value, 0.0)).astype(jnp.bfloat16).reshape(2, rows // 2, H)
            else:
                lifted[src] = value

        def lift_mine(s):
            lift(0, s * up_rows + y * (up_rows // 2), up_rows // 2)

        def lift_others(s, last=False):
            up_others(s)
            lift(0, s * up_rows + (1 - y) * (up_rows // 2), up_rows // 2, last=last)

        def relay(name, j, k):
            s = unit[name]
            dn_landed(s, j, k)
            dn_copy(s, j, k, None, MATE if name == "outer" else ACROSS).start()

        def relay_up(s, p, where):
            up_copy(s, p, None, where).start()

        tok_load.wait()
        lax.fori_loop(0, 4, lambda q, carry: (normalise(0, q), carry)[1], 0)

        for p in range(UM):
            up_landed(outer, p)
            relay_up(outer, p, MATE)
            up_landed(mate, p)
            if p < UM - VIA_MATE:
                relay_up(mate, p, ACROSS)
            if p >= UM - BESIDE:
                relay_up(outer, p, ACROSS)
            if p == 1:
                lift(0, z * up_rows, up_rows, first=True)
        for p in range(UM - VIA_MATE, UM):
            up_copy(z, p, None, MATE, True).start()
        for j in range(DC):
            dn_loads[j].wait()
            for k in range(DM):
                dn_copy(z, j, k, dn_own(j, mine_dn + k), MATE).start()
        lift_mine(outer)
        lift_mine(mate)

        beside, beyond = x * 2 + 1 - core, (1 - x) * 2 + core
        corner = (1 - x) * 2 + 1 - core

        def pass_beyond(b):
            tok_copy(TP + b, beyond, b, tok_slot(beyond, b), ASIDE).wait_recv()
            tok_copy(2 * TP + 1, beyond, b, tok_slot(beyond, b), PARTNER).start()

        for b in range(TP):
            for p in range(b * UM // TP, (b + 1) * UM // TP):
                up_landed(far, p)
                relay_up(far, p, ACROSS)
            tok_copy(b, t, b, tok_slot(t, b), INNER).wait_recv()
            tok_copy(TP + b, t, b, tok_slot(t, b), ASIDE).start()
            tok_copy(2 * TP, t, b, tok_slot(t, b), PARTNER).start()
            if b > 1:
                pass_beyond(b - 2)
        normalise(1, t)
        lift_mine(far)
        tok_all(2 * TP, beside)
        normalise(1, beside)
        pass_beyond(TP - 2)
        pass_beyond(TP - 1)
        normalise(1, beyond)
        tok_all(2 * TP + 1, corner)
        normalise(1, corner)
        due = []
        for name, first in (("mate", 32.0), ("outer", 34.0), ("far", 44.0)):
            due += [(first + 1.4 * q, name, q // DM, q % DM) for q in range(DC * DM)]
        due.sort()

        def relays(until):
            while due and due[0][0] <= until:
                relay(*due.pop(0)[1:])

        relays(33)
        near = jnp.where(z < n // 2, 0, n // 2) * up_rows
        lift_others(outer)
        relays(34.5)
        lift(1, near, 2 * up_rows, first=True)
        relays(35.8)
        lift_others(mate)
        lift_others(far, last=True)

        def a_copy(i, src):
            return remote(asend.at[i, src], arecv.at[i, src], a_send.at[0], a_recv.at[i, src], PARTNER)

        def b_copy(i, src):
            return remote(bsend.at[i, src], brecv.at[i, src], b_send.at[0], b_recv.at[i, src], ASIDE)

        joining, finishing = [], []

        def join(left=0):
            while len(joining) > left:
                i, src = joining.pop(0)
                a_copy(i, src).wait_recv()

                def added(to):
                    return part[i % 2, src, core, to] + arecv[i, src, to].astype(jnp.float32)

                if src == 1 and i in DIRECT:
                    for to in (0, 1):
                        dsend[i, to] = added(to).astype(jnp.bfloat16)
                        d_copy(i, to, x).start()
                else:
                    bsend[i, src] = added(1 - x).astype(jnp.bfloat16)
                    b_copy(i, src).start()
                    keep[i, src] = added(x)
                    finishing.append((i, src))

        def finish(left):
            while len(finishing) > left:
                i, src = finishing.pop(0)
                q = column(i)
                b_copy(i, src).wait_recv()
                res = own_tokens(src, q) + keep[i, src] + brecv[i, src].astype(jnp.float32)
                outv[src, q] = res.astype(jnp.bfloat16)
                (own_copy if src == 0 else out_copy)(i).start()

        def give(i, src):
            asend[i, src] = part[i % 2, src, 1 - core].astype(jnp.bfloat16)
            a_copy(i, src).start()

        def compute(i, src):
            product = jnp.dot(hid[src].reshape(rows, H), dnw[column(i)], preferred_element_type=jnp.float32)
            part[i % 2, src] = product.reshape(2, 2, own_rows, CW)
            give(i, src)
            join()
            joining.append((i, src))
            finish(LAG)

        def both(i):
            name, j = ORDER[i]
            if name != "inner":
                dn_others(unit[name], j)
            product = jnp.dot(hid[...].reshape(2 * rows, H), dnw[column(i)], preferred_element_type=jnp.float32)
            part[i % 2] = product.reshape(2, 2, 2, own_rows, CW)
            give(i, 1)
            give(i, 0)
            join()
            joining.extend([(i, 1), (i, 0)])
            finish(LAG)

        relays(37)
        compute(0, 0)
        compute(1, 0)
        relays(38)
        lift(1, (n // 2) * up_rows - near, 2 * up_rows, last=True)
        join()
        relays(39.5)
        compute(0, 1)
        relays(40.5)
        compute(1, 1)
        relays(41.5)
        join()
        relays(43)
        both(2)
        relays(44.5)
        join()
        relays(46)
        both(3)
        relays(47.5)
        join()
        relays(50)
        both(4)
        relays(51.5)
        join()
        relays(52.5)
        both(5)
        relays(54)
        join()
        relays(99)
        both(6)
        both(7)
        join()
        finish(0)

        ups = 2 * UM + VIA_MATE + (UM - VIA_MATE) + UM + BESIDE
        sent(upw.at[pl.ds(0, ups * piece), :], up_send, MATE)
        sent(dnw.at[pl.ds(0, 2 * DC)], dn_send, MATE)
        sent(tok.at[0, pl.ds(0, 3 * own_rows), :], t_send, MATE)
        sent(asend, a_send, PARTNER)
        sent(bsend.at[pl.ds(0, chunks - passed // 2)], b_send, ASIDE)
        sent(outv.at[1, pl.ds(0, chunks - passed)], o_send, OUTER)
        sent(dsend.at[pl.ds(0, passed)], d_send, OUTER)
        own_done(chunks)


def fused(n, tokens, norm_gain, up_weight, down_weight):
    rows, D = tokens.shape
    up_rows, H = up_weight.shape
    CW = down_weight.shape[1] // DN_CHUNKS
    chunks = n * DN_CHUNKS
    own_rows = rows // 4
    bf, f32 = jnp.bfloat16, jnp.float32
    dma = pltpu.SemaphoreType.DMA
    return pl.pallas_call(
        functools.partial(kernel, n),
        out_shape=jax.ShapeDtypeStruct((own_rows, D), bf),
        in_specs=[pl.BlockSpec(memory_space=pl.ANY)] * 4,
        out_specs=pl.BlockSpec(memory_space=pl.ANY),
        scratch_shapes=[
            pltpu.VMEM((1, D), f32),
            pltpu.VMEM((2, rows, D), bf),
            pltpu.VMEM((2, rows, D), bf),
            pltpu.VMEM((n * up_rows, H), bf),
            pltpu.VMEM((chunks, H, CW), bf),
            pltpu.VMEM((2, rows, H), f32),
            pltpu.VMEM((2, 2, rows // 2, H), bf),
            pltpu.VMEM((2, 2, 2, 2, own_rows, CW), f32),
            pltpu.VMEM((chunks, 2, 2, own_rows, CW), bf),
            pltpu.VMEM((chunks, 2, 2, own_rows, CW), bf),
            pltpu.VMEM((chunks, 2, own_rows, CW), bf),
            pltpu.VMEM((chunks, 2, own_rows, CW), bf),
            pltpu.VMEM((chunks, 2, own_rows, CW), f32),
            pltpu.VMEM((2, chunks, own_rows, CW), bf),
            pltpu.VMEM((chunks, 2, own_rows, CW), bf),
            pltpu.VMEM((chunks, 2, own_rows, CW), bf),
            dma((1,)),
            dma((n * (UP_PIECES // 2 + 1),)),
            dma((1,)),
            dma((chunks * (DN_PIECES // 2 + 1),)),
            dma((1,)),
            dma((2 * TOK_PIECES + 2,)),
            dma((1,)),
            dma((chunks, 2)),
            dma((1,)),
            dma((chunks, 2)),
            dma((1,)),
            dma((chunks,)),
            dma((1,)),
            dma((chunks,)),
            dma((1,)),
            dma((3 + DN_CHUNKS,)),
        ],
        compiler_params=pltpu.CompilerParams(
            collective_id=0, has_side_effects=True, vmem_limit_bytes=53 * 1024 * 1024
        ),
    )(tokens, norm_gain.reshape(1, D), up_weight, down_weight)


def fits(mesh, tokens, up_weight, down_weight):
    n = mesh.shape["fs"]
    rows = tokens.shape[0] // (mesh.shape["rep"] * n)
    columns = down_weight.shape[1] // n
    depth = up_weight.shape[0] // n
    hidden = up_weight.shape[1] // mesh.shape["tp"]
    return (
        mesh.shape["rep"] == 2
        and mesh.shape["tp"] == 4
        and n == 4
        and columns % (128 * DN_CHUNKS) == 0
        and depth % (UP_PIECES * 16) == 0
        and depth % 128 == 0
        and hidden % (16 * DN_PIECES) == 0
        and hidden % 128 == 0
        and rows % (4 * 16 * TOK_PIECES) == 0
        and rows <= 512
        and hidden <= 1024
        and tokens.shape[1] <= 2048
    )


def solution(mesh):
    placed = (P(("rep", "fs"), None), P(), P("fs", "tp"), P("tp", "fs"))

    def layer(tokens, norm_gain, up_weight, down_weight):
        if fits(mesh, tokens, up_weight, down_weight):
            body = functools.partial(fused, mesh.shape["fs"])
        else:
            body = shards
        return jax.shard_map(
            body, mesh=mesh, in_specs=placed, out_specs=P(("rep", "fs", "tp"), None), check_vma=False
        )(tokens, norm_gain, up_weight, down_weight)

    return layer
```

time: 82.8 us -> 72.3 us (0.87)
  Pallas kernels: 81.1 us -> 70.6 us
    pallas_call x1, Pallas kernels: 81.1 us -> 70.6 us  [fused(): pl.pallas_call(functools.partial(kernel, n), out_shape=jax.ShapeDtypeStru...]
where the time goes in v2:
time: 72.3 us; the launch traced here: 72.1 us
  Pallas kernels  70.6 us (98%)
  local copies, waits for them, and re-layouts  1.49 us (2%)
    pallas_call x1, Pallas kernels, fused(): pl.pallas_call(functools.partial(kernel, n), out_shape=jax.ShapeDtypeStru...  70.6 us
    unnamed x3, local copies, waits for them, and re-layouts  1.49 us

profile of v2, /device:TPU:0, one launch (start us, length us, event | category | flops | bytes accessed | tf_op | source)
XLA Modules:
  0.0 72.1 jit_solution(6355910371461848279)
XLA Ops:
  0.0 0.0 copy-start
  0.0 0.7 copy-done
  0.7 70.6 %shard_map.46 = bf16[128,2048]{1,0:T(8,128)(2,1)S(1)} custom-call(bf16[512,2048]{1,0:T(8,128)(2,1)} %tok_hbm.1, f32[1,2048]{1,0:T(1,128)S(1)} %bitcast.1, bf16[512,1024]{1,0:T(8,128)(2,1)} %up_hbm.1, bf16[1024,512]{1,0:T(8,128)(2,1)} %dn_hbm.1), custom_call_target="tpu_custom_call" | custom-call | tf_op jit(solution)/shard_map/pallas_call | solution.py:461
  71.3 0.8 %copy.6 = bf16[128,2048]{1,0:T(8,128)(2,1)} copy(bf16[128,2048]{1,0:T(8,128)(2,1)S(1)} %shard_map.46) | data formatting | bytes 1048576
Async XLA Ops:
  0.0 0.7 copy-start

commit v3 on v2

--- a/solution.py
+++ b/solution.py
@@ -19,7 +19,7 @@
     ("inner", 0), ("inner", 1), ("mate", 0), ("mate", 1),
     ("outer", 0), ("far", 0), ("outer", 1), ("far", 1),
 )
-DIRECT = (1, 3, 5, 7)
+DIRECT = (1, 4, 5, 7)
 
 
 def shards(tokens, norm_gain, up_weight, down_weight):
@@ -73,6 +73,7 @@
     UM, DM = UP // 2, DP // 2
     piece, depth, band = up_rows // UP, H // DP, own_rows // TP
     chunks = n * DC
+    HALF = CW // 2
 
     is_outer = (z == 0) | (z == n - 1)
     outer = jnp.where(z < n // 2, 0, n - 1)
@@ -103,11 +104,19 @@
     def up_own(p):
         return up_hbm.at[pl.ds(pl.multiple_of(p * piece, piece), piece), :]
 
-    def dn_slot(s, j, k):
-        return dnw.at[s * DC + j, pl.ds(pl.multiple_of(k * depth, depth), depth), :]
-
-    def dn_own(j, k):
-        return dn_hbm.at[pl.ds(pl.multiple_of(k * depth, depth), depth), pl.ds(j * CW, CW)]
+    def dn_part(j, k, other):
+        side = ((1 - y) if other else y) * (H // 2)
+        if j < DC - 1:
+            return pl.ds(pl.multiple_of(side + k * depth, depth), depth), pl.ds(0, CW)
+        return pl.ds(pl.multiple_of(side + k % 2 * 2 * depth, 2 * depth), 2 * depth), pl.ds(k // 2 * HALF, HALF)
+
+    def dn_slot(s, j, k, other=False):
+        r, c = dn_part(j, k, other)
+        return dnw.at[s * DC + j, r, c]
+
+    def dn_own(j, k, other=False):
+        r, c = dn_part(j, k, other)
+        return dn_hbm.at[r, pl.ds(j * CW + c.start, c.size)]
 
     def up_copy(s, p, src, where, other=False):
         slot = up_slot(s, p + ((1 - y) if other else y) * UM)
@@ -115,11 +124,13 @@
         recv = up_recv.at[n * UM + s] if crossing else up_recv.at[s * UM + p]
         return remote(slot if src is None else src, slot, up_send.at[0], recv, where)
 
-    def dn_copy(s, j, k, src, where, other=False):
-        slot = dn_slot(s, j, k + ((1 - y) if other else y) * DM)
-        crossing = where is ACROSS or other
-        recv = dn_recv.at[chunks * DM + s * DC + j] if crossing else dn_recv.at[(s * DC + j) * DM + k]
-        return remote(slot if src is None else src, slot, dn_send.at[0], recv, where)
+    def dn_copy(s, j, k, where, other=False, stored=False):
+        slot = dn_slot(s, j, k, other)
+        if where is ACROSS or other:
+            recv = dn_recv.at[chunks * DM + s * (DC + 1) + j + (k // 2 if j == DC - 1 else 0)]
+        else:
+            recv = dn_recv.at[(s * DC + j) * DM + k]
+        return remote(dn_own(j, k, other) if stored else slot, slot, dn_send.at[0], recv, where)
 
     def up_landed(s, p):
         up_copy(s, p, None, MATE).wait_recv()
@@ -130,12 +141,12 @@
         remote(ref, ref, up_send.at[0], up_recv.at[n * UM + s], MATE).wait_recv()
 
     def dn_landed(s, j, k):
-        dn_copy(s, j, k, None, MATE).wait_recv()
-
-    def dn_others(s, j):
-        half = H // 2
-        ref = dnw.at[s * DC + j, pl.ds(pl.multiple_of((1 - y) * half, half), half), :]
-        remote(ref, ref, dn_send.at[0], dn_recv.at[chunks * DM + s * DC + j], MATE).wait_recv()
+        dn_copy(s, j, k, MATE).wait_recv()
+
+    def dn_others(s, j, h=0):
+        cols = pl.ds(h * HALF, HALF) if j == DC - 1 else pl.ds(0, CW)
+        ref = dnw.at[s * DC + j, pl.ds(pl.multiple_of((1 - y) * (H // 2), H // 2), H // 2), cols]
+        remote(ref, ref, dn_send.at[0], dn_recv.at[chunks * DM + s * (DC + 1) + j + h], MATE).wait_recv()
 
     def tok_slot(q, b):
         return tok.at[1, pl.ds(pl.multiple_of(q * own_rows + b * band, band), band), :]
@@ -150,29 +161,38 @@
     def sent(ref, sem, where):
         remote(ref, ref, sem.at[0], sem.at[0], where).wait_send()
 
-    def out_cols(q):
-        return out_hbm.at[:, pl.ds(pl.multiple_of(q * CW, CW), CW)]
-
     def column(i):
         return unit[ORDER[i][0]] * DC + ORDER[i][1]
 
-    def own_copy(i):
+    def cut(h):
+        return pl.ds(0, CW) if h is None else pl.ds(h * HALF, HALF)
+
+    def mark(i, h):
+        return chunks if h == 1 else i
+
+    def out_part(q, h):
+        start = pl.multiple_of(q * CW + (h or 0) * HALF, HALF)
+        return out_hbm.at[:, pl.ds(start, CW if h is None else HALF)]
+
+    def own_copy(i, h=None):
         q = column(i)
-        return pltpu.make_async_copy(outv.at[0, q], out_cols(q), own_sem.at[0])
+        return pltpu.make_async_copy(outv.at[0, q, :, cut(h)], out_part(q, h), own_sem.at[0])
 
     def own_done(count):
         width = pl.ds(0, count * CW)
         pltpu.make_async_copy(tok.at[0, pl.ds(0, own_rows), width], out_hbm.at[:, width], own_sem.at[0]).wait()
 
-    def out_copy(i):
+    def out_copy(i, h=None):
         q = column(i)
-        return remote(outv.at[1, q], out_cols(q), o_send.at[0], o_recv.at[i], OUTER)
-
-    def d_copy(i, to, of):
-        return remote(dsend.at[i, to], drecv.at[i, of], d_send.at[0], d_recv.at[i], at(y, outer, to * 2 + core))
-
-    def d_landed(i):
-        remote(dsend.at[i], drecv.at[i], d_send.at[0], d_recv.at[i], INNER).wait_recv()
+        return remote(outv.at[1, q, :, cut(h)], out_part(q, h), o_send.at[0], o_recv.at[mark(i, h)], OUTER)
+
+    def d_copy(i, to, of, h=None):
+        return remote(dsend.at[i, to, :, cut(h)], drecv.at[i, of, :, cut(h)], d_send.at[0], d_recv.at[mark(i, h)],
+                      at(y, outer, to * 2 + core))
+
+    def d_landed(i, h=None):
+        ref = drecv.at[i, :, :, cut(h)]
+        remote(ref, ref, d_send.at[0], d_recv.at[mark(i, h)], INNER).wait_recv()
 
     barrier = pltpu.get_barrier_semaphore()
 
@@ -181,12 +201,12 @@
             pl.semaphore_signal(barrier, inc=1, device_id=peer, device_id_type=pl.DeviceIdType.MESH)
 
     mine_up, other_up = y * UM, (1 - y) * UM
-    mine_dn, other_dn = y * DM, (1 - y) * DM
     passed = len(DIRECT)
     own_block = pl.ds(pl.multiple_of(t * own_rows, own_rows), own_rows)
 
-    def own_tokens(src, q):
-        return tok[src, own_block, pl.ds(pl.multiple_of(q * CW, CW), CW)].astype(jnp.float32)
+    def own_tokens(src, q, h=None):
+        start = pl.multiple_of(q * CW + (h or 0) * HALF, HALF)
+        return tok[src, own_block, pl.ds(start, CW if h is None else HALF)].astype(jnp.float32)
 
     @pl.when(is_outer)
     def _():
@@ -206,22 +226,21 @@
             tok_copy(b, t, b, own, INNER).start()
         for p in range(UM - BESIDE):
             up_copy(z, p, None, INNER, True).start()
-        for j in range(DC):
-            for k in range(DM):
-                dn_copy(z, j, k, dn_own(j, mine_dn + k), INNER).start()
-        for j in range(DC):
-            for k in range(DM):
-                dn_copy(z, j, k, dn_own(j, other_dn + k), INNER, True).start()
+        for other in (False, True):
+            for j in range(DC):
+                for k in range(DM):
+                    dn_copy(z, j, k, INNER, other, True).start()
         load.wait()
         for i in range(chunks):
-            if i in DIRECT:
-                d_landed(i)
-                q = column(i)
-                res = own_tokens(0, q) + drecv[i, 0].astype(jnp.float32) + drecv[i, 1].astype(jnp.float32)
-                outv[0, q] = res.astype(jnp.bfloat16)
-                own_copy(i).start()
-            else:
-                out_copy(i).wait_recv()
+            for h in (0, 1) if i == chunks - 1 else (None,):
+                if i in DIRECT:
+                    d_landed(i, h)
+                    q, c = column(i), cut(h)
+                    res = own_tokens(0, q, h) + drecv[i, 0, :, c].astype(jnp.float32)
+                    outv[0, q, :, c] = (res + drecv[i, 1, :, c].astype(jnp.float32)).astype(jnp.bfloat16)
+                    own_copy(i, h).start()
+                else:
+                    out_copy(i, h).wait_recv()
         sent(upw.at[pl.ds(0, (2 * UM - BESIDE) * piece), :], up_send, INNER)
         sent(dnw.at[pl.ds(0, DC)], dn_send, INNER)
         sent(tok.at[0, pl.ds(0, own_rows), :], t_send, INNER)
@@ -276,7 +295,7 @@
         def relay(name, j, k):
             s = unit[name]
             dn_landed(s, j, k)
-            dn_copy(s, j, k, None, MATE if name == "outer" else ACROSS).start()
+            dn_copy(s, j, k, MATE if name == "outer" else ACROSS).start()
 
         def relay_up(s, p, where):
             up_copy(s, p, None, where).start()
@@ -299,7 +318,7 @@
         for j in range(DC):
             dn_loads[j].wait()
             for k in range(DM):
-                dn_copy(z, j, k, dn_own(j, mine_dn + k), MATE).start()
+                dn_copy(z, j, k, MATE, False, True).start()
         lift_mine(outer)
         lift_mine(mate)
 
@@ -319,6 +338,15 @@
             tok_copy(2 * TP, t, b, tok_slot(t, b), PARTNER).start()
             if b > 1:
                 pass_beyond(b - 2)
+        due = []
+        for name, first in (("mate", 32.2), ("outer", 34.0), ("far", 43.5)):
+            due += [(first + 1.4 * q, name, q // DM, q % DM) for q in range(DC * DM)]
+        due.sort()
+
+        def relays(until):
+            while due and due[0][0] <= until:
+                relay(*due.pop(0)[1:])
+
         normalise(1, t)
         lift_mine(far)
         tok_all(2 * TP, beside)
@@ -326,116 +354,134 @@
         pass_beyond(TP - 2)
         pass_beyond(TP - 1)
         normalise(1, beyond)
+        relays(33)
         tok_all(2 * TP + 1, corner)
         normalise(1, corner)
-        due = []
-        for name, first in (("mate", 32.0), ("outer", 34.0), ("far", 44.0)):
-            due += [(first + 1.4 * q, name, q // DM, q % DM) for q in range(DC * DM)]
-        due.sort()
-
-        def relays(until):
-            while due and due[0][0] <= until:
-                relay(*due.pop(0)[1:])
-
-        relays(33)
         near = jnp.where(z < n // 2, 0, n // 2) * up_rows
         lift_others(outer)
-        relays(34.5)
+        relays(33.7)
         lift(1, near, 2 * up_rows, first=True)
-        relays(35.8)
+        relays(35)
         lift_others(mate)
+        relays(35.5)
         lift_others(far, last=True)
-
-        def a_copy(i, src):
-            return remote(asend.at[i, src], arecv.at[i, src], a_send.at[0], a_recv.at[i, src], PARTNER)
-
-        def b_copy(i, src):
-            return remote(bsend.at[i, src], brecv.at[i, src], b_send.at[0], b_recv.at[i, src], ASIDE)
+        relays(36.5)
+        lift(1, (n // 2) * up_rows - near, 2 * up_rows, last=True)
+        relays(37.8)
+
+        def a_copy(i, src, h=None):
+            return remote(asend.at[i, src, :, :, cut(h)], arecv.at[i, src, :, :, cut(h)],
+                          a_send.at[0], a_recv.at[mark(i, h), src], PARTNER)
+
+        def b_copy(i, src, h=None):
+            return remote(bsend.at[i, src, :, cut(h)], brecv.at[i, src, :, cut(h)],
+                          b_send.at[0], b_recv.at[mark(i, h), src], ASIDE)
 
         joining, finishing = [], []
 
         def join(left=0):
             while len(joining) > left:
-                i, src = joining.pop(0)
-                a_copy(i, src).wait_recv()
+                i, src, h = joining.pop(0)
+                c = cut(h)
+                a_copy(i, src, h).wait_recv()
 
                 def added(to):
-                    return part[i % 2, src, core, to] + arecv[i, src, to].astype(jnp.float32)
+                    return part[i % 2, src, core, to, :, c] + arecv[i, src, to, :, c].astype(jnp.float32)
 
                 if src == 1 and i in DIRECT:
-                    for to in (0, 1):
-                        dsend[i, to] = added(to).astype(jnp.bfloat16)
-                        d_copy(i, to, x).start()
+                    for to in (1 - x, x):
+                        dsend[i, to, :, c] = added(to).astype(jnp.bfloat16)
+                        d_copy(i, to, x, h).start()
                 else:
-                    bsend[i, src] = added(1 - x).astype(jnp.bfloat16)
-                    b_copy(i, src).start()
-                    keep[i, src] = added(x)
-                    finishing.append((i, src))
+                    bsend[i, src, :, c] = added(1 - x).astype(jnp.bfloat16)
+                    b_copy(i, src, h).start()
+                    keep[i, src, :, c] = added(x)
+                    finishing.append((i, src, h))
+
+        def pick(*item):
+            joining.remove(item)
+            joining.insert(0, item)
+            join(len(joining) - 1)
 
         def finish(left):
             while len(finishing) > left:
-                i, src = finishing.pop(0)
-                q = column(i)
-                b_copy(i, src).wait_recv()
-                res = own_tokens(src, q) + keep[i, src] + brecv[i, src].astype(jnp.float32)
-                outv[src, q] = res.astype(jnp.bfloat16)
-                (own_copy if src == 0 else out_copy)(i).start()
-
-        def give(i, src):
-            asend[i, src] = part[i % 2, src, 1 - core].astype(jnp.bfloat16)
-            a_copy(i, src).start()
-
-        def compute(i, src):
-            product = jnp.dot(hid[src].reshape(rows, H), dnw[column(i)], preferred_element_type=jnp.float32)
-            part[i % 2, src] = product.reshape(2, 2, own_rows, CW)
-            give(i, src)
-            join()
-            joining.append((i, src))
-            finish(LAG)
-
-        def both(i):
+                i, src, h = finishing.pop(0)
+                q, c = column(i), cut(h)
+                b_copy(i, src, h).wait_recv()
+                res = own_tokens(src, q, h) + keep[i, src, :, c] + brecv[i, src, :, c].astype(jnp.float32)
+                outv[src, q, :, c] = res.astype(jnp.bfloat16)
+                (own_copy if src == 0 else out_copy)(i, h).start()
+
+        def give(i, src, h=None):
+            c = cut(h)
+            asend[i, src, :, :, c] = part[i % 2, src, 1 - core, :, :, c].astype(jnp.bfloat16)
+            a_copy(i, src, h).start()
+            joining.append((i, src, h))
+
+        def arrive(i):
             name, j = ORDER[i]
             if name != "inner":
-                dn_others(unit[name], j)
-            product = jnp.dot(hid[...].reshape(2 * rows, H), dnw[column(i)], preferred_element_type=jnp.float32)
-            part[i % 2] = product.reshape(2, 2, 2, own_rows, CW)
-            give(i, 1)
-            give(i, 0)
-            join()
-            joining.extend([(i, 1), (i, 0)])
-            finish(LAG)
-
-        relays(37)
-        compute(0, 0)
-        compute(1, 0)
-        relays(38)
-        lift(1, (n // 2) * up_rows - near, 2 * up_rows, last=True)
+                for h in (0, 1) if j == DC - 1 else (0,):
+                    dn_others(unit[name], j, h)
+
+        def compute(i, src, h=None):
+            block = dnw[column(i), :, cut(h)]
+            for side in (0, 1):
+                product = jnp.dot(hid[src, side], block, preferred_element_type=jnp.float32)
+                part[i % 2, src, side, :, :, cut(h)] = product.reshape(2, own_rows, block.shape[1])
+            give(i, src, h)
+
+        def both(i, h=None):
+            block = dnw[column(i), :, cut(h)]
+            for src in (0, 1):
+                product = jnp.dot(hid[src].reshape(rows, H), block, preferred_element_type=jnp.float32)
+                part[i % 2, src, :, :, :, cut(h)] = product.reshape(2, 2, own_rows, block.shape[1])
+            give(i, 1, h)
+            give(i, 0, h)
+
+        both(0)
+        relays(39.2)
+        both(1)
+        join(2)
+        relays(40.6)
         join()
-        relays(39.5)
-        compute(0, 1)
-        relays(40.5)
-        compute(1, 1)
-        relays(41.5)
+        relays(42)
+        arrive(2)
+        both(2)
+        relays(43.6)
         join()
-        relays(43)
-        both(2)
-        relays(44.5)
+        relays(46.4)
+        finish(3)
+        arrive(3)
+        both(3)
+        relays(47.8)
+        finish(2)
         join()
-        relays(46)
-        both(3)
-        relays(47.5)
+        relays(49.2)
+        finish(2)
+        arrive(4)
+        both(4)
+        relays(50.6)
         join()
-        relays(50)
-        both(4)
-        relays(51.5)
-        join()
-        relays(52.5)
+        relays(52)
+        relays(99)
+        arrive(5)
         both(5)
-        relays(54)
-        join()
-        relays(99)
-        both(6)
-        both(7)
+        finish(1)
+        arrive(6)
+        compute(6, 1)
+        join(1)
+        compute(6, 0)
+        finish(2)
+        dn_others(far, DC - 1, 0)
+        both(7, 0)
+        pick(6, 1, None)
+        dn_others(far, DC - 1, 1)
+        compute(7, 1, 1)
+        pick(7, 1, 0)
+        compute(7, 0, 1)
+        pick(7, 1, 1)
+        finish(0)
         join()
         finish(0)
 
@@ -483,17 +529,17 @@
             dma((1,)),
             dma((n * (UP_PIECES // 2 + 1),)),
             dma((1,)),
-            dma((chunks * (DN_PIECES // 2 + 1),)),
+            dma((chunks * (DN_PIECES // 2 + 1) + n,)),
             dma((1,)),
             dma((2 * TOK_PIECES + 2,)),
             dma((1,)),
-            dma((chunks, 2)),
-            dma((1,)),
-            dma((chunks, 2)),
-            dma((1,)),
-            dma((chunks,)),
-            dma((1,)),
-            dma((chunks,)),
+            dma((chunks + 1, 2)),
+            dma((1,)),
+            dma((chunks + 1, 2)),
+            dma((1,)),
+            dma((chunks + 1,)),
+            dma((1,)),
+            dma((chunks + 1,)),
             dma((1,)),
             dma((3 + DN_CHUNKS,)),
         ],
@@ -513,7 +559,7 @@
         mesh.shape["rep"] == 2
         and mesh.shape["tp"] == 4
         and n == 4
-        and columns % (128 * DN_CHUNKS) == 0
+        and columns % (256 * DN_CHUNKS) == 0
         and depth % (UP_PIECES * 16) == 0
         and depth % 128 == 0
         and hidden % (16 * DN_PIECES) == 0

time: 72.3 us -> 69.6 us (0.963)
  Pallas kernels: 70.6 us -> 67.9 us
    pallas_call x1, Pallas kernels: 70.6 us -> 67.9 us  [fused(): pl.pallas_call(functools.partial(kernel, n), out_shape=jax.ShapeDtypeStru...]
where the time goes in v3:
time: 69.6 us; the launch traced here: 69.4 us
  Pallas kernels  67.9 us (98%)
  local copies, waits for them, and re-layouts  1.49 us (2%)
    pallas_call x1, Pallas kernels, fused(): pl.pallas_call(functools.partial(kernel, n), out_shape=jax.ShapeDtypeStru...  67.9 us
    unnamed x3, local copies, waits for them, and re-layouts  1.49 us

profile of v3, /device:TPU:0, one launch (start us, length us, event | category | flops | bytes accessed | tf_op | source)
XLA Modules:
  0.0 69.4 jit_solution(15511660808539891338)
XLA Ops:
  0.0 0.0 copy-start
  0.0 0.7 %copy-done = f32[2048]{0:T(1024)S(1)} copy-done((f32[2048]{0:T(1024)S(1)}, f32[2048]{0:T(1024)}, u32[]{:S(2)}) %copy-start) | copy-done | bytes 8216
  0.7 67.9 %shard_map.46 = bf16[128,2048]{1,0:T(8,128)(2,1)S(1)} custom-call(bf16[512,2048]{1,0:T(8,128)(2,1)} %tok_hbm.1, f32[1,2048]{1,0:T(1,128)S(1)} %bitcast.1, bf16[512,1024]{1,0:T(8,128)(2,1)} %up_hbm.1, bf16[1024,512]{1,0:T(8,128)(2,1)} %dn_hbm.1), custom_call_target="tpu_custom_call" | custom-call | tf_op jit(solution)/shard_map/pallas_call | solution.py:507
  68.6 0.8 %copy.6 = bf16[128,2048]{1,0:T(8,128)(2,1)} copy(bf16[128,2048]{1,0:T(8,128)(2,1)S(1)} %shard_map.46) | data formatting | bytes 1048576
Async XLA Ops:
  0.0 0.7 %copy-start = (f32[2048]{0:T(1024)S(1)}, f32[2048]{0:T(1024)}, u32[]{:S(2)}) copy-start(f32[2048]{0:T(1024)} %param.5) | copy-start | bytes 24580

commit v4 on v3

--- a/solution.py
+++ b/solution.py
@@ -19,7 +19,7 @@
     ("inner", 0), ("inner", 1), ("mate", 0), ("mate", 1),
     ("outer", 0), ("far", 0), ("outer", 1), ("far", 1),
 )
-DIRECT = (1, 4, 5, 7)
+DIRECT = (1, 2, 3, 4, 5, 7)
 
 
 def shards(tokens, norm_gain, up_weight, down_weight):
@@ -61,7 +61,7 @@
     n, tok_hbm, gain_hbm, up_hbm, dn_hbm, out_hbm,
     gain_ref, tok, nrm, upw, dnw, lifted, hid, part, asend, arecv, bsend, brecv, keep, outv, dsend, drecv,
     up_send, up_recv, dn_send, dn_recv, t_send, t_recv,
-    a_send, a_recv, b_send, b_recv, o_send, o_recv, d_send, d_recv, own_sem, local,
+    a_send, a_recv, b_send, b_recv, o_send, o_recv, d_send, own_sem, local,
 ):
     y, z, t = lax.axis_index("rep"), lax.axis_index("fs"), lax.axis_index("tp")
     x, core = t // 2, t % 2
@@ -118,35 +118,42 @@
         r, c = dn_part(j, k, other)
         return dn_hbm.at[r, pl.ds(j * CW + c.start, c.size)]
 
-    def up_copy(s, p, src, where, other=False):
+    def rank(s, where, here=False):
+        plane = z if here or where is ACROSS else mate if where is MATE else inner
+        return s - jnp.where(s > plane, 1, 0)
+
+    def up_copy(s, p, src, where, other=False, here=False):
         slot = up_slot(s, p + ((1 - y) if other else y) * UM)
         crossing = where is ACROSS or other
-        recv = up_recv.at[n * UM + s] if crossing else up_recv.at[s * UM + p]
+        g = rank(s, where, here)
+        recv = up_recv.at[(n - 1) * UM + g] if crossing else up_recv.at[g * UM + p]
         return remote(slot if src is None else src, slot, up_send.at[0], recv, where)
 
-    def dn_copy(s, j, k, where, other=False, stored=False):
+    def dn_copy(s, j, k, where, other=False, stored=False, here=False):
         slot = dn_slot(s, j, k, other)
+        g = rank(s, where, here)
         if where is ACROSS or other:
-            recv = dn_recv.at[chunks * DM + s * (DC + 1) + j + (k // 2 if j == DC - 1 else 0)]
+            recv = dn_recv.at[(n - 1) * DC * DM + g * (DC + 1) + j + (k // 2 if j == DC - 1 else 0)]
         else:
-            recv = dn_recv.at[(s * DC + j) * DM + k]
+            recv = dn_recv.at[(g * DC + j) * DM + k]
         return remote(dn_own(j, k, other) if stored else slot, slot, dn_send.at[0], recv, where)
 
     def up_landed(s, p):
-        up_copy(s, p, None, MATE).wait_recv()
+        up_copy(s, p, None, MATE, here=True).wait_recv()
 
     def up_others(s):
         half = up_rows // 2
         ref = upw.at[pl.ds(pl.multiple_of(s * up_rows + (1 - y) * half, half), half), :]
-        remote(ref, ref, up_send.at[0], up_recv.at[n * UM + s], MATE).wait_recv()
+        remote(ref, ref, up_send.at[0], up_recv.at[(n - 1) * UM + rank(s, MATE, True)], MATE).wait_recv()
 
     def dn_landed(s, j, k):
-        dn_copy(s, j, k, MATE).wait_recv()
+        dn_copy(s, j, k, MATE, here=True).wait_recv()
 
     def dn_others(s, j, h=0):
         cols = pl.ds(h * HALF, HALF) if j == DC - 1 else pl.ds(0, CW)
         ref = dnw.at[s * DC + j, pl.ds(pl.multiple_of((1 - y) * (H // 2), H // 2), H // 2), cols]
-        remote(ref, ref, dn_send.at[0], dn_recv.at[chunks * DM + s * (DC + 1) + j + h], MATE).wait_recv()
+        recv = dn_recv.at[(n - 1) * DC * DM + rank(s, MATE, True) * (DC + 1) + j + h]
+        remote(ref, ref, dn_send.at[0], recv, MATE).wait_recv()
 
     def tok_slot(q, b):
         return tok.at[1, pl.ds(pl.multiple_of(q * own_rows + b * band, band), band), :]
@@ -187,12 +194,12 @@
         return remote(outv.at[1, q, :, cut(h)], out_part(q, h), o_send.at[0], o_recv.at[mark(i, h)], OUTER)
 
     def d_copy(i, to, of, h=None):
-        return remote(dsend.at[i, to, :, cut(h)], drecv.at[i, of, :, cut(h)], d_send.at[0], d_recv.at[mark(i, h)],
+        return remote(dsend.at[i, to, :, cut(h)], drecv.at[i, of, :, cut(h)], d_send.at[0], o_recv.at[mark(i, h)],
                       at(y, outer, to * 2 + core))
 
     def d_landed(i, h=None):
         ref = drecv.at[i, :, :, cut(h)]
-        remote(ref, ref, d_send.at[0], d_recv.at[mark(i, h)], INNER).wait_recv()
+        remote(ref, ref, d_send.at[0], o_recv.at[mark(i, h)], INNER).wait_recv()
 
     barrier = pltpu.get_barrier_semaphore()
 
@@ -527,9 +534,9 @@
             pltpu.VMEM((chunks, 2, own_rows, CW), bf),
             pltpu.VMEM((chunks, 2, own_rows, CW), bf),
             dma((1,)),
-            dma((n * (UP_PIECES // 2 + 1),)),
-            dma((1,)),
-            dma((chunks * (DN_PIECES // 2 + 1) + n,)),
+            dma(((n - 1) * (UP_PIECES // 2 + 1),)),
+            dma((1,)),
+            dma(((n - 1) * (DN_CHUNKS * (DN_PIECES // 2 + 1) + 1),)),
             dma((1,)),
             dma((2 * TOK_PIECES + 2,)),
             dma((1,)),
@@ -539,7 +546,6 @@
             dma((1,)),
             dma((chunks + 1,)),
             dma((1,)),
-            dma((chunks + 1,)),
             dma((1,)),
             dma((3 + DN_CHUNKS,)),
         ],

time: 69.6 us -> 68.6 us (0.986)
  Pallas kernels: 67.9 us -> 66.9 us
    pallas_call x1, Pallas kernels: 67.9 us -> 66.9 us  [fused(): pl.pallas_call(functools.partial(kernel, n), out_shape=jax.ShapeDtypeStru...]
where the time goes in v4:
time: 68.6 us; the launch traced here: 68.4 us
  Pallas kernels  66.9 us (98%)
  local copies, waits for them, and re-layouts  1.49 us (2%)
    pallas_call x1, Pallas kernels, fused(): pl.pallas_call(functools.partial(kernel, n), out_shape=jax.ShapeDtypeStru...  66.9 us
    unnamed x3, local copies, waits for them, and re-layouts  1.49 us

profile of v4, /device:TPU:0, one launch (start us, length us, event | category | flops | bytes accessed | tf_op | source)
XLA Modules:
  0.0 68.4 jit_solution(11728128713998903926)
XLA Ops:
  0.0 0.0 copy-start
  0.0 0.7 %copy-done = f32[2048]{0:T(1024)S(1)} copy-done((f32[2048]{0:T(1024)S(1)}, f32[2048]{0:T(1024)}, u32[]{:S(2)}) %copy-start) | copy-done | bytes 8216
  0.7 66.9 %shard_map.46 = bf16[128,2048]{1,0:T(8,128)(2,1)S(1)} custom-call(bf16[512,2048]{1,0:T(8,128)(2,1)} %tok_hbm.1, f32[1,2048]{1,0:T(1,128)S(1)} %bitcast.1, bf16[512,1024]{1,0:T(8,128)(2,1)} %up_hbm.1, bf16[1024,512]{1,0:T(8,128)(2,1)} %dn_hbm.1), custom_call_target="tpu_custom_call" | custom-call | tf_op jit(solution)/shard_map/pallas_call | solution.py:514
  67.6 0.8 %copy.6 = bf16[128,2048]{1,0:T(8,128)(2,1)} copy(bf16[128,2048]{1,0:T(8,128)(2,1)S(1)} %shard_map.46) | data formatting | bytes 1048576
Async XLA Ops:
  0.0 0.7 %copy-start = (f32[2048]{0:T(1024)S(1)}, f32[2048]{0:T(1024)}, u32[]{:S(2)}) copy-start(f32[2048]{0:T(1024)} %param.5) | copy-start | bytes 24580

commit v5 on v4

--- a/solution.py
+++ b/solution.py
@@ -462,10 +462,8 @@
         arrive(3)
         both(3)
         relays(47.8)
-        finish(2)
         join()
         relays(49.2)
-        finish(2)
         arrive(4)
         both(4)
         relays(50.6)
@@ -474,7 +472,6 @@
         relays(99)
         arrive(5)
         both(5)
-        finish(1)
         arrive(6)
         compute(6, 1)
         join(1)

time: 68.6 us -> 68.6 us (level)
  no operation moved by 1% of the time
where the time goes in v5:
time: 68.6 us; the launch traced here: 68.4 us
  Pallas kernels  66.9 us (98%)
  local copies, waits for them, and re-layouts  1.49 us (2%)
    pallas_call x1, Pallas kernels, fused(): pl.pallas_call(functools.partial(kernel, n), out_shape=jax.ShapeDtypeStru...  66.9 us
    unnamed x3, local copies, waits for them, and re-layouts  1.49 us

profile of v5, /device:TPU:0, one launch (start us, length us, event | category | flops | bytes accessed | tf_op | source)
XLA Modules:
  0.0 68.4 jit_solution(18266133200780599264)
XLA Ops:
  0.0 0.0 copy-start
  0.0 0.7 %copy-done = f32[2048]{0:T(1024)S(1)} copy-done((f32[2048]{0:T(1024)S(1)}, f32[2048]{0:T(1024)}, u32[]{:S(2)}) %copy-start) | copy-done | bytes 8216
  0.7 66.9 %shard_map.46 = bf16[128,2048]{1,0:T(8,128)(2,1)S(1)} custom-call(bf16[512,2048]{1,0:T(8,128)(2,1)} %tok_hbm.1, f32[1,2048]{1,0:T(1,128)S(1)} %bitcast.1, bf16[512,1024]{1,0:T(8,128)(2,1)} %up_hbm.1, bf16[1024,512]{1,0:T(8,128)(2,1)} %dn_hbm.1), custom_call_target="tpu_custom_call" | custom-call | tf_op jit(solution)/shard_map/pallas_call | solution.py:511
  67.6 0.8 %copy.6 = bf16[128,2048]{1,0:T(8,128)(2,1)} copy(bf16[128,2048]{1,0:T(8,128)(2,1)S(1)} %shard_map.46) | data formatting | bytes 1048576
Async XLA Ops:
  0.0 0.7 %copy-start = (f32[2048]{0:T(1024)S(1)}, f32[2048]{0:T(1024)}, u32[]{:S(2)}) copy-start(f32[2048]{0:T(1024)} %param.5) | copy-start | bytes 24580
